TPU v7x, 256 devices: a whole 4x4x8 slice. The times are simulated.
256 devices in a mesh: sp: 16 (over y, x), tp: 16 (over z, core).
Axes of the slice: x: 4, y: 4, z: 8, core: 2. Of those that a mesh axis runs over, the one named last changes fastest.
Arguments:
- query_vectors: bfloat16 [16384, 16, 128], P('sp', 'tp'), may hold values from -6 to 6
- key_vectors: bfloat16 [16384, 16, 128], P('sp', 'tp'), may hold values from -6 to 6
- value_vectors: bfloat16 [16384, 16, 128], P('sp', 'tp'), may hold values from -6 to 6
- out_gate: bfloat16 [16384, 16, 128], P('sp', 'tp'), may hold values from -6 to 6
- decay_rate: float32 [2, 16], P(None, 'tp'), may hold values from 0 to 1
- decay_pre: float32 [2, 16, 16384], P(None, 'tp', 'sp'), may hold values from -6 to 6
- decay_shock: float32 [2, 16, 16384], P(None, 'tp', 'sp'), may hold values from -2 to 0
- beta_pre: float32 [2, 16, 16384], P(None, 'tp', 'sp'), may hold values from -12 to 0
- head_gain: float32 [128], replicated, may hold values from 0.1 to 1.9
- w_out: bfloat16 [2048, 2048], P('tp'), may hold values from -0.125 to 0.125
- tokens: bfloat16 [16384, 2048], P(('sp', 'tp')), may hold values from -6 to 6
- norm_gain: float32 [2048], replicated, may hold values from 0.1 to 1.9
- experts_pick: int32 [16384, 2], P(('sp', 'tp')), may hold values from 0 to 15, as said below
- pair_logits: float32 [16384, 2], P(('sp', 'tp')), may hold values from -6 to 6
- group_logits: float32 [16384, 8], P(('sp', 'tp')), may hold values from -6 to 6
- expert_gate: bfloat16 [16, 2048, 2048], P('sp', None, 'tp'), may hold values from -0.125 to 0.125
- expert_up: bfloat16 [16, 2048, 2048], P('sp', None, 'tp'), may hold values from -0.125 to 0.125
- expert_down: bfloat16 [16, 2048, 2048], P('sp', None, 'tp'), may hold values from -0.5 to 0.5
Outputs:
- layer_out: bfloat16 [16384, 2048], P(('sp', 'tp'))
Inputs may be any that keep to these rules, and one draw needn't show every extreme that they name: `experts_pick`: each token names two different experts of one group of 2 consecutive experts. The 64 tokens of one device fall 8 into each group. At most 8 tokens of one device name any one expert, and in every draw every expert is named by 8 tokens of every device.
All inputs are finite; a program needn't handle non-finite values.
Results may differ from a plain program's by a relative error of at most 0.02.
Values may be sent and summed in bfloat16 or wider, within the bound.
No kernel may reach another device: no remote copies, remote signals or barrier semaphores. Data moves between devices by JAX's collectives and lax.ppermute only.
A program may use at most 128 MiB of HBM per device.

v0:
```python
import jax
import jax.numpy as jnp
from jax import lax
from jax.sharding import Mesh
from jax.sharding import PartitionSpec as P

BLOCK = 64
GROUP_SIZE = 2
SP = ("sp_0", "sp_1")
SP_TP = ("sp_0", "sp_1", "tp")
NORM_EPSILON = 1e-06


def neutral_like(x, identity):
    return jax.tree.map(
        lambda part, zero: jnp.zeros_like(part) + jnp.asarray(zero, part.dtype), x, identity
    )


def prefix_by_axis(x, axes, combine, identity, reverse):
    before = start = neutral_like(x, identity)
    subtotal = x
    for axis in reversed(axes):
        peers, position = (lax.axis_size(axis), lax.axis_index(axis))
        pieces = jax.tree.map(
            lambda part, kind: lax.all_gather(part.astype(kind), axis),
            subtotal,
            (jnp.bfloat16, jnp.bfloat16),
        )
        inside, subtotal = (start, start)
        for k in reversed(range(peers)) if reverse else range(peers):
            passed = k > position if reverse else k < position
            subtotal = combine(
                subtotal, jax.tree.map(lambda part, own: part[k].astype(own.dtype), pieces, x)
            )
            inside = jax.tree.map(lambda new, old: jnp.where(passed, new, old), subtotal, inside)
        before = combine(inside, before)
    return before


def unit_rows(vectors):
    return vectors * lax.rsqrt(jnp.sum(vectors * vectors, axis=-1, keepdims=True) + NORM_EPSILON)


def block_sweep(queries, key_rows, value_rows, log_decay, beta_rate, start_state):
    length, value_width = value_rows.shape
    blocks = length // BLOCK
    query_blocks = queries.reshape(blocks, BLOCK, queries.shape[1])
    key_blocks = key_rows.reshape(blocks, BLOCK, key_rows.shape[1])
    value_blocks = value_rows.reshape(blocks, BLOCK, value_width)
    cumulative = jnp.cumsum(log_decay.reshape(blocks, BLOCK), axis=1)
    beta_blocks = beta_rate.reshape(blocks, BLOCK)
    position = jnp.arange(BLOCK)
    lower_mask = position[:, None] >= position[None, :]
    strict = position[:, None] > position[None, :]
    spread = cumulative[:, :, None] - cumulative[:, None, :]
    within = jnp.where(lower_mask, jnp.exp(jnp.where(lower_mask, spread, 0.0)), 0.0)
    scaled_keys = key_blocks * beta_blocks[:, :, None]
    lower_matrix = jnp.where(
        strict, jnp.einsum("nid,njd->nij", scaled_keys, key_blocks) * within, 0.0
    )
    identity = jnp.eye(BLOCK, dtype=jnp.float32)
    right_side = jnp.concatenate(
        [value_blocks * beta_blocks[:, :, None], scaled_keys * jnp.exp(cumulative)[:, :, None]],
        axis=2,
    )
    solved = jax.scipy.linalg.solve_triangular(
        lower_matrix + identity, right_side, lower=True, unit_diagonal=True
    )
    fresh_values = solved[:, :, :value_width]
    corrections = solved[:, :, value_width:]
    scores = jnp.einsum("nid,njd->nij", query_blocks, key_blocks) * within
    query_decayed = query_blocks * jnp.exp(cumulative)[:, :, None]
    block_total = cumulative[:, -1]
    decayed_keys = key_blocks * jnp.exp(block_total[:, None] - cumulative)[:, :, None]

    def advance(carried, inputs):
        values_in, fix_rows, query_in, key_in, score_in, total_in = inputs
        updated = values_in - jnp.dot(fix_rows, carried)
        output = jnp.dot(query_in, carried) + jnp.dot(score_in, updated)
        carried = carried * jnp.exp(total_in) + jnp.dot(key_in.T, updated)
        return (carried, output)

    final_state, outputs = lax.scan(
        advance,
        start_state,
        (fresh_values, corrections, query_decayed, decayed_keys, scores, block_total),
    )
    return (outputs.reshape(length, value_width), final_state)


def shards(
    query_vectors,
    key_vectors,
    value_vectors,
    out_gate,
    decay_rate,
    decay_pre,
    decay_shock,
    beta_pre,
    head_gain,
    w_out,
    tokens,
    norm_gain,
    experts_pick,
    pair_logits,
    group_logits,
    expert_gate,
    expert_up,
    expert_down,
):
    per_head_width = query_vectors.shape[2]
    queries = unit_rows(
        jnp.transpose(query_vectors.astype(jnp.float32), (1, 0, 2))
    ) * per_head_width ** (-0.5)
    keyset = unit_rows(jnp.transpose(key_vectors.astype(jnp.float32), (1, 0, 2)))
    valueset = jnp.transpose(value_vectors.astype(jnp.float32), (1, 0, 2))
    padded_values = jnp.concatenate([valueset, jnp.zeros_like(keyset)], axis=2)
    log_decay = jnp.moveaxis(
        -decay_rate[:, :, None] * jax.nn.softplus(decay_pre) + decay_shock, 1, 0
    )
    beta_rate = jnp.moveaxis(jax.nn.sigmoid(beta_pre), 1, 0)
    identity = jnp.eye(per_head_width, dtype=jnp.float32)
    opening = jnp.concatenate(
        [jnp.zeros((per_head_width, per_head_width), jnp.float32), identity], axis=1
    )

    def one_head(query_head, key_head, value_head, decay_head, beta_head):
        forward_result, ahead_end = block_sweep(
            query_head, key_head, value_head, decay_head[0], beta_head[0], opening
        )
        trailing_part, behind_end = block_sweep(
            query_head[::-1],
            key_head[::-1],
            value_head[::-1],
            decay_head[1, ::-1],
            beta_head[1, ::-1],
            opening,
        )
        return (forward_result, trailing_part[::-1], ahead_end, behind_end)

    forward_result, trailing_part, ahead_end, behind_end = jax.vmap(one_head)(
        queries, keyset, padded_values, log_decay, beta_rate
    )
    forward_shift = ahead_end[:, :, per_head_width:]
    forward_add = ahead_end[:, :, :per_head_width]
    backward_shift = behind_end[:, :, per_head_width:]
    backward_add = behind_end[:, :, :per_head_width]

    def compose(earlier, later):
        return (
            jnp.einsum("hij,hjk->hik", later[0], earlier[0]),
            jnp.einsum("hij,hjv->hiv", later[0], earlier[1]) + later[1],
        )

    neutral = (jnp.broadcast_to(identity, forward_shift.shape), jnp.zeros_like(forward_add))
    forward_carried = prefix_by_axis((forward_shift, forward_add), SP, compose, neutral, False)[1]
    backward_carried = prefix_by_axis((backward_shift, backward_add), SP, compose, neutral, True)[1]
    joined = (
        forward_result[:, :, :per_head_width]
        + trailing_part[:, :, :per_head_width]
        + jnp.einsum("qfc,qcj->qfj", forward_result[:, :, per_head_width:], forward_carried)
        + jnp.einsum("qfc,qcj->qfj", trailing_part[:, :, per_head_width:], backward_carried)
    )
    joined = jnp.transpose(joined, (1, 0, 2))
    head_scale = lax.rsqrt(jnp.mean(joined * joined, axis=-1, keepdims=True) + NORM_EPSILON)
    mixed_heads = (
        joined * head_scale * head_gain * jax.nn.silu(out_gate.astype(jnp.float32))
    ).astype(jnp.bfloat16)
    mixed_heads = mixed_heads.reshape(joined.shape[0], joined.shape[1] * per_head_width)
    local_rows = tokens.shape[0]
    part_sum = jnp.dot(mixed_heads, w_out, preferred_element_type=jnp.float32).astype(jnp.bfloat16)
    branch_sum = lax.psum_scatter(
        lax.optimization_barrier(part_sum).astype(jnp.float32).astype(jnp.bfloat16),
        "tp",
        scatter_dimension=0,
        tiled=True,
    ).astype(jnp.float32)
    residual = tokens.astype(jnp.float32) + branch_sum
    normed = (
        residual
        * lax.rsqrt(jnp.mean(residual * residual, axis=-1, keepdims=True) + NORM_EPSILON)
        * norm_gain
    ).astype(jnp.bfloat16)
    group_count = group_logits.shape[1]
    group_exp = jnp.exp(group_logits)
    group_share = group_exp / jnp.sum(group_exp, axis=-1, keepdims=True)
    group_index_of = experts_pick[:, 0] // GROUP_SIZE
    group_weight = jnp.sum(
        jnp.where(jnp.arange(group_count)[None, :] == group_index_of[:, None], group_share, 0.0),
        axis=1,
    )
    pair_exp = jnp.exp(pair_logits)
    route_weight = pair_exp / jnp.sum(pair_exp, axis=-1, keepdims=True) * group_weight[:, None]
    capacity = local_rows // group_count
    expert_count = lax.axis_size(SP)
    expert_marks = jnp.sum(
        (
            experts_pick[:, :, None] == jnp.arange(expert_count, dtype=jnp.int32)[None, None, :]
        ).astype(jnp.int32),
        axis=1,
    )
    earlier = jnp.cumsum(expert_marks, axis=0) - expert_marks
    slot_place = experts_pick * capacity + jnp.take_along_axis(earlier, experts_pick, axis=1)
    slot_index = jnp.arange(expert_count * capacity, dtype=jnp.int32)[:, None]
    chooser = (
        (slot_index == slot_place[None, :, 0]) | (slot_index == slot_place[None, :, 1])
    ).astype(jnp.bfloat16)
    outgoing = jnp.dot(chooser, normed, preferred_element_type=jnp.float32).astype(jnp.bfloat16)
    outgoing = outgoing.reshape(expert_count, capacity, normed.shape[1])
    arrived = lax.all_to_all(outgoing, SP, split_axis=0, concat_axis=0, tiled=True)
    source_count, slot_count, model_width = arrived.shape
    row_count = source_count * slot_count
    flat_rows = arrived.reshape(row_count, model_width)
    part_rows = lax.all_gather(flat_rows, "tp", axis=0, tiled=True)
    gate_out = jnp.dot(part_rows, expert_gate[0], preferred_element_type=jnp.float32)
    up_out = jnp.dot(part_rows, expert_up[0], preferred_element_type=jnp.float32)
    hidden = (jax.nn.silu(gate_out) * up_out).astype(jnp.bfloat16)
    product = lax.dot_general(
        hidden, expert_down[0], (((1,), (1,)), ((), ())), preferred_element_type=jnp.float32
    ).astype(jnp.bfloat16)
    summed_out = lax.psum_scatter(
        lax.optimization_barrier(product).astype(jnp.float32).astype(jnp.bfloat16),
        "tp",
        scatter_dimension=0,
        tiled=True,
    )
    expert_rows = summed_out.reshape(source_count, slot_count, model_width)
    results = lax.all_to_all(expert_rows, SP, split_axis=0, concat_axis=0, tiled=True)
    gathered = results.reshape(expert_count * capacity, normed.shape[1])
    chosen = gathered[slot_place]
    mixture = jnp.einsum("tk,tkd->td", route_weight, chosen.astype(jnp.float32))
    return (residual + mixture).astype(jnp.bfloat16)


def solution(mesh):
    finer = Mesh(mesh.devices.reshape(4, 4, mesh.shape["tp"]), ("sp_0", "sp_1", "tp"))
    in_specs = (
        P(SP, "tp", None),
        P(SP, "tp", None),
        P(SP, "tp", None),
        P(SP, "tp", None),
        P(None, "tp"),
        P(None, "tp", SP),
        P(None, "tp", SP),
        P(None, "tp", SP),
        P(),
        P("tp", None),
        P(SP_TP, None),
        P(),
        P(SP_TP, None),
        P(SP_TP, None),
        P(SP_TP, None),
        P(SP, None, "tp"),
        P(SP, None, "tp"),
        P(SP, None, "tp"),
    )
    out_specs = P(SP_TP, None)
    return jax.shard_map(
        shards, mesh=finer, in_specs=in_specs, out_specs=out_specs, check_vma=False
    )
```

profile of v0, /device:TPU:2, one launch (start us, length us, event | category | flops | bytes accessed | tf_op | source)
XLA Modules:
  0.0 675.1 jit_solution(16698587801744514501)
XLA Ops:
  12.5 78.6 %custom-call.6 = f32[1,16,1,64,64]{3,4,2,1,0:T(8,128)S(1)} custom-call(f32[1,16,1,64,64]{4,3,2,1,0:T(8,128)S(1)} %fusion.59), custom_call_target="InvertDiagBlocksLowerTriangular" | custom-call | tf_op jit(solution)/shard_map/vmap(jit(_solve_triangular))/vmap()/triangular_solve | solution.py:67
  101.2 3.4 rev.17
  107.1 79.4 %custom-call.7 = f32[1,16,1,64,64]{3,4,2,1,0:T(8,128)S(1)} custom-call(f32[1,16,1,64,64]{4,3,2,1,0:T(8,128)} %fusion.62), custom_call_target="InvertDiagBlocksLowerTriangular" | custom-call | tf_op jit(solution)/shard_map/vmap(jit(_solve_triangular))/vmap()/triangular_solve | solution.py:67
  192.6 53.2 %while.25 = (s32[]{:T(128)}, f32[1,128,256]{2,1,0:T(8,128)S(1)}, f32[16,1,64,256]{3,2,1,0:T(8,128)S(1)}, f32[16,1]{0,1:T(1,128)S(1)}, bf16[16,1,64,128]{3,2,1,0:...) while((s32[]{:T(128)}, f32[1,128,256]{2,1,0:T(8,128)S(1)}, ...), condition=%wide.region_7.9_spmd, body=%wide.region_6.8_spmd.sunk | while | flops 14794754 | bytes 952445 | solution.py:84
  248.9 54.2 %while.24 = (s32[]{:T(128)}, f32[1,128,256]{2,1,0:T(8,128)S(1)}, f32[16,1,64,256]{3,2,1,0:T(8,128)S(1)}, f32[16,1]{0,1:T(1,128)S(1)}, bf16[16,1,64,128]{3,2,1,0:...) while((s32[]{:T(128)}, f32[1,128,256]{2,1,0:T(8,128)S(1)}, ...), condition=%wide.region_4.6_spmd, body=%wide.region_3.5_spmd.sunk | while | flops 14794754 | bytes 952445 | solution.py:84
  303.1 12.1 %all-gather = bf16[4,128,128]{2,1,0:T(8,128)(2,1)S(1)} all-gather(bf16[1,128,128]{2,1,0:T(8,128)(2,1)S(1)} %get-tuple-element.234), channel_id=2, replica_groups=mesh['sp_0'=4,'sp_1'=4,'tp'=16] {'sp_1'}, dimensions={0}, use_global_device_ids=true | all-gather | bytes 163840 | tf_op jit(solution)/shard_map/all_gather | solution.py:26
  316.3 12.5 %all-gather.1 = bf16[512,128]{1,0:T(8,128)(2,1)S(1)} all-gather(bf16[128,128]{1,0:T(8,128)(2,1)S(1)} %fusion.226), channel_id=3, replica_groups=mesh['sp_0'=4,'sp_1'=4,'tp'=16] {'sp_0'}, dimensions={0}, use_global_device_ids=true | all-gather | bytes 163840 | tf_op jit(solution)/shard_map/all_gather | solution.py:26
  328.8 12.0 %all-gather.2 = bf16[4,128,128]{2,1,0:T(8,128)(2,1)S(1)} all-gather(bf16[1,128,128]{2,1,0:T(8,128)(2,1)S(1)} %get-tuple-element.235), channel_id=4, replica_groups=mesh['sp_0'=4,'sp_1'=4,'tp'=16] {'sp_1'}, dimensions={0}, use_global_device_ids=true | all-gather | bytes 163840 | tf_op jit(solution)/shard_map/all_gather | solution.py:26
  342.0 12.0 %all-gather.3 = bf16[512,128]{1,0:T(8,128)(2,1)S(1)} all-gather(bf16[128,128]{1,0:T(8,128)(2,1)S(1)} %convolution_add_fusion.15), channel_id=5, replica_groups=mesh['sp_0'=4,'sp_1'=4,'tp'=16] {'sp_0'}, dimensions={0}, use_global_device_ids=true | all-gather | bytes 163840 | tf_op jit(solution)/shard_map/all_gather | solution.py:26
  355.1 12.0 %all-gather.4 = bf16[4,128,128]{2,1,0:T(8,128)(2,1)S(1)} all-gather(bf16[1,128,128]{2,1,0:T(8,128)(2,1)S(1)} %get-tuple-element.236), channel_id=6, replica_groups=mesh['sp_0'=4,'sp_1'=4,'tp'=16] {'sp_1'}, dimensions={0}, use_global_device_ids=true | all-gather | bytes 163840 | tf_op jit(solution)/shard_map/all_gather | solution.py:26
  368.7 12.2 %all-gather.5 = bf16[512,128]{1,0:T(8,128)(2,1)S(1)} all-gather(bf16[128,128]{1,0:T(8,128)(2,1)S(1)} %fusion.229), channel_id=7, replica_groups=mesh['sp_0'=4,'sp_1'=4,'tp'=16] {'sp_0'}, dimensions={0}, use_global_device_ids=true | all-gather | bytes 163840 | tf_op jit(solution)/shard_map/all_gather | solution.py:26
  380.9 12.0 %all-gather.6 = bf16[4,128,128]{2,1,0:T(8,128)(2,1)S(1)} all-gather(bf16[1,128,128]{2,1,0:T(8,128)(2,1)S(1)} %get-tuple-element.237), channel_id=8, replica_groups=mesh['sp_0'=4,'sp_1'=4,'tp'=16] {'sp_1'}, dimensions={0}, use_global_device_ids=true | all-gather | bytes 163840 | tf_op jit(solution)/shard_map/all_gather | solution.py:26
  394.5 12.0 %all-gather.7 = bf16[512,128]{1,0:T(8,128)(2,1)S(1)} all-gather(bf16[128,128]{1,0:T(8,128)(2,1)S(1)} %convolution_add_fusion.6), channel_id=9, replica_groups=mesh['sp_0'=4,'sp_1'=4,'tp'=16] {'sp_0'}, dimensions={0}, use_global_device_ids=true | all-gather | bytes 163840 | tf_op jit(solution)/shard_map/all_gather | solution.py:26
  410.1 3.9 slice.185
  415.2 2.0 convolution_bitcast_fusion.2
  421.6 4.3 convolution_convert_fusion.1
  428.6 61.8 %reduce-scatter.3.cloned.1.call-done = bf16[64,2048]{1,0:T(8,128)(2,1)} async-done(((bf16[1024,2048]{1,0:T(8,128)(2,1)}), bf16[64,2048]{1,0:T(8,128)(2,1)}) %reduce-scatter.3.cloned.1.call-update) | async-done | bytes 262160 | tf_op jit(solution)/shard_map/reduce_scatter | solution.py:173
  493.0 16.0 %all_to_all.10 = bf16[16,8,2048]{2,1,0:T(8,128)(2,1)} all-to-all(bf16[16,8,2048]{2,1,0:T(8,128)(2,1)S(1)} %fusion.37), channel_id=1, replica_groups=mesh['sp_0'=4,'sp_1'=4,'tp'=16] {'sp_0','sp_1'}, dimensions={0} | all-to-all | bytes 1048576 | tf_op jit(solution)/shard_map/all_to_all | solution.py:211
  509.0 52.6 %all-gather.10.cloned.1.call-done = bf16[2048,2048]{1,0:T(8,128)(2,1)} async-done(((bf16[128,2048]{1,0:T(8,128)(2,1)}), bf16[2048,2048]{1,0:T(8,128)(2,1)}) %all-gather.10.cloned.1.call-update) | async-done | bytes 8388624 | tf_op jit(solution)/shard_map/all_gather | solution.py:215
  561.6 5.7 fusion.86
  567.3 12.8 %convolution_convert_fusion = bf16[2048,2048]{1,0:T(8,128)(2,1)} fusion(bf16[2048,2048]{1,0:T(8,128)(2,1)} %all-gather.10.cloned.1.call-done, f32[2048,128]{1,0:T(8,128)S(1)} %fusion.86, bf16[1,2048,128]{2,1,0:T(8,128)(2,1)S(1)} %copy-done, bf16[1,2048,128]{2,1,0:T(8,128)(2,1)S(1)} %copy-done.6), kind=kOutput, calls=%fused_computation.46 | convolution fusion | flops 2153250816 | bytes 18874368 | tf_op jit(solution)/shard_map/dot_general | solution.py:219
  580.9 68.7 %reduce-scatter.5.cloned.1.call-done = bf16[128,2048]{1,0:T(8,128)(2,1)} async-done(((bf16[2048,2048]{1,0:T(8,128)(2,1)}), bf16[128,2048]{1,0:T(8,128)(2,1)}) %reduce-scatter.5.cloned.1.call-update) | async-done | bytes 524304 | tf_op jit(solution)/shard_map/reduce_scatter | solution.py:222
  649.6 7.3 %all-to-all-start.1 = ((bf16[16,8,2048]{2,1,0:T(8,128)(2,1)}), bf16[16,8,2048]{2,1,0:T(8,128)(2,1)S(1)}, u32[]{:S(2)}, u32[]{:S(2)}) async-start(bf16[16,8,2048]{2,1,0:T(8,128)(2,1)} %bitcast.435), calls=%async_computation.3 | async-start | bytes 1048576 | tf_op jit(solution)/shard_map/all_to_all | solution.py:229
  657.3 8.3 %all-to-all-done.1 = bf16[16,8,2048]{2,1,0:T(8,128)(2,1)S(1)} async-done(((bf16[16,8,2048]{2,1,0:T(8,128)(2,1)}), bf16[16,8,2048]{2,1,0:T(8,128)(2,1)S(1)}, u32[]{:S(2)}, u32[]{:S(2)}) %all-to-all-start.1) | async-done | bytes 524320 | tf_op jit(solution)/shard_map/all_to_all | solution.py:229
  (405 shorter events, 158.7 us)
Async XLA Ops:
  6.5 560.8 %copy-start = (bf16[1,2048,128]{2,1,0:T(8,128)(2,1)S(1)}, bf16[1,2048,128]{2,1,0:T(8,128)(2,1)}, u32[]{:S(2)}) copy-start(bf16[1,2048,128]{2,1,0:T(8,128)(2,1)} %param.41) | copy-start | bytes 1572868
  6.5 483.9 %reduce-scatter.3.cloned.1.call-start = ((), (), s32[]{:S(2)}) async-start(), calls=%async_computation.4 | async-start | bytes 4456448 | tf_op jit(solution)/shard_map/reduce_scatter | solution.py:173
  7.8 83.5 %copy-start.22 = (bf16[1024,1,128]{2,0,1:T(8,128)(2,1)S(1)}, bf16[1024,1,128]{2,0,1:T(8,128)(2,1)}, u32[]{:S(2)}) copy-start(bf16[1024,1,128]{2,0,1:T(8,128)(2,1)} %param.26) | copy-start | bytes 786436
  8.8 82.5 %copy-start.41 = (f32[64,64]{1,0:T(8,128)}, f32[64,64]{1,0:T(8,128)S(1)}, u32[]{:S(2)}) copy-start(f32[64,64]{1,0:T(8,128)S(1)} %get-tuple-element.256) | copy-start | bytes 49156
  8.8 82.5 %copy-start.47 = (pred[64,64]{1,0:T(8,128)(4,1)}, pred[64,64]{1,0:T(8,128)(4,1)S(1)}, u32[]{:S(2)}) copy-start(pred[64,64]{1,0:T(8,128)(4,1)S(1)} %get-tuple-element.255) | copy-start | bytes 12292
  8.9 82.5 %copy-start.42 = (f32[64,64]{1,0:T(8,128)}, f32[64,64]{1,0:T(8,128)S(1)}, u32[]{:S(2)}) copy-start(f32[64,64]{1,0:T(8,128)S(1)} %fusion.185) | copy-start | bytes 49156
  11.3 80.0 %copy-start.49 = (pred[64,64]{1,0:T(8,128)(4,1)}, pred[64,64]{1,0:T(8,128)(4,1)S(1)}, u32[]{:S(2)}) copy-start(pred[64,64]{1,0:T(8,128)(4,1)S(1)} %get-tuple-element.253) | copy-start | bytes 12292
  11.8 79.6 %copy-start.51 = (f32[16]{0:T(128)}, f32[16]{0:T(128)S(1)}, u32[]{:S(2)}) copy-start(f32[16]{0:T(128)S(1)} %slice_reduce_fusion.1) | copy-start | bytes 196
  105.1 81.7 %copy-start.53 = (f32[16]{0:T(128)}, f32[16]{0:T(128)S(1)}, u32[]{:S(2)}) copy-start(f32[16]{0:T(128)S(1)} %slice_reduce_fusion) | copy-start | bytes 196
  316.0 12.8 %copy-start.23 = (bf16[128,128]{1,0:T(8,128)(2,1)}, bf16[128,128]{1,0:T(8,128)(2,1)S(1)}, u32[]{:S(2)}) copy-start(bf16[128,128]{1,0:T(8,128)(2,1)S(1)} %fusion.228) | copy-start | bytes 98308
  341.0 27.1 %copy-start.10 = (bf16[128,128]{1,0:T(8,128)(2,1)}, bf16[128,128]{1,0:T(8,128)(2,1)S(1)}, u32[]{:S(2)}) copy-start(bf16[128,128]{1,0:T(8,128)(2,1)S(1)} %convolution_add_fusion.18) | copy-start | bytes 98308
  341.8 26.2 %copy-start.16 = (bf16[128,128]{1,0:T(8,128)(2,1)}, bf16[128,128]{1,0:T(8,128)(2,1)S(1)}, u32[]{:S(2)}) copy-start(bf16[128,128]{1,0:T(8,128)(2,1)S(1)} %convolution_add_fusion.16) | copy-start | bytes 98308
  342.0 26.1 %copy-start.12 = (bf16[128,128]{1,0:T(8,128)(2,1)}, bf16[128,128]{1,0:T(8,128)(2,1)S(1)}, u32[]{:S(2)}) copy-start(bf16[128,128]{1,0:T(8,128)(2,1)S(1)} %convolution_add_fusion.15) | copy-start | bytes 98308
  354.0 52.7 %copy-start.7 = (bf16[512,128]{1,0:T(8,128)(2,1)}, bf16[512,128]{1,0:T(8,128)(2,1)S(1)}, u32[]{:S(2)}) copy-start(bf16[512,128]{1,0:T(8,128)(2,1)S(1)} %all-gather.3) | copy-start | bytes 393220
  368.7 24.2 %copy-start.31 = (bf16[128,128]{1,0:T(8,128)(2,1)}, bf16[128,128]{1,0:T(8,128)(2,1)S(1)}, u32[]{:S(2)}) copy-start(bf16[128,128]{1,0:T(8,128)(2,1)S(1)} %fusion.229) | copy-start | bytes 98308
  380.8 27.9 %copy-start.8 = (bf16[512,128]{1,0:T(8,128)(2,1)}, bf16[512,128]{1,0:T(8,128)(2,1)S(1)}, u32[]{:S(2)}) copy-start(bf16[512,128]{1,0:T(8,128)(2,1)S(1)} %all-gather.5) | copy-start | bytes 393220
  426.0 135.6 %all-gather.10.cloned.1.call-start = ((), (), s32[]{:S(2)}) async-start(), calls=%async_computation.5 | async-start | bytes 8912896 | tf_op jit(solution)/shard_map/all_gather | solution.py:215
  427.1 63.4 %copy-start.1 = (bf16[64,2048]{1,0:T(8,128)(2,1)S(1)}, bf16[64,2048]{1,0:T(8,128)(2,1)}, u32[]{:S(2)}) copy-start(bf16[64,2048]{1,0:T(8,128)(2,1)} %param.34) | copy-start | bytes 786436
  427.1 64.5 %copy-start.46 = (f32[2048]{0:T(1024)S(1)}, f32[2048]{0:T(1024)}, u32[]{:S(2)}) copy-start(f32[2048]{0:T(1024)} %param.35) | copy-start | bytes 24580
  428.6 133.0 %copy-start.56 = (bf16[1,2048,128]{2,1,0:T(8,128)(2,1)S(1)}, bf16[1,2048,128]{2,1,0:T(8,128)(2,1)}, u32[]{:S(2)}) copy-start(bf16[1,2048,128]{2,1,0:T(8,128)(2,1)} %param.39) | copy-start | bytes 1572868
  508.9 58.4 %copy-start.6 = (bf16[1,2048,128]{2,1,0:T(8,128)(2,1)S(1)}, bf16[1,2048,128]{2,1,0:T(8,128)(2,1)}, u32[]{:S(2)}) copy-start(bf16[1,2048,128]{2,1,0:T(8,128)(2,1)} %param.40) | copy-start | bytes 1572868
  509.0 140.7 %reduce-scatter.5.cloned.1.call-start = ((), (), s32[]{:S(2)}) async-start(), calls=%async_computation.6 | async-start | bytes 8912896 | tf_op jit(solution)/shard_map/reduce_scatter | solution.py:222
  580.2 76.7 %copy-start.55 = (f32[64,2]{0,1:T(2,128)S(1)}, f32[64,2]{0,1:T(2,128)}, u32[]{:S(2)}) copy-start(f32[64,2]{0,1:T(2,128)} %param.37) | copy-start | bytes 1540
  649.6 16.1 %all-to-all-start.1 = ((bf16[16,8,2048]{2,1,0:T(8,128)(2,1)}), bf16[16,8,2048]{2,1,0:T(8,128)(2,1)S(1)}, u32[]{:S(2)}, u32[]{:S(2)}) async-start(bf16[16,8,2048]{2,1,0:T(8,128)(2,1)} %bitcast.435), calls=%async_computation.3 | async-start | bytes 1048576 | tf_op jit(solution)/shard_map/all_to_all | solution.py:229
  (37 other events, 164.5 us)
Sparse Core Ops, SparseCore 0:
  426.1 64.3 reduce-scatter.2
  509.1 52.4 all-gather.9
  580.3 69.2 reduce-scatter.4
where the time goes:
time: 682 us; the launch traced here: 675 us
  waiting for transfers between devices  192 us (28%)
  other arithmetic  171 us (25%)
  matrix products  132 us (19%)
  blocking collectives  113 us (17%)
  local copies, waits for them, and re-layouts  46 us (7%)
  between operations  14.1 us (2%)
  starting transfers between devices  7.36 us (1%)
    another operation x5, other arithmetic, block_sweep(): jax.scipy.linalg.solve_triangular(lower_matrix + identity, right_side, lo...  158 us
    all_gather x8, blocking collectives, prefix_by_axis(): lax.all_gather(part.astype(kind), axis)  96.7 us
    reduce_scatter x1, waiting for transfers between devices, shards(): lax.psum_scatter(lax.optimization_barrier(product).astype(jnp.float32).as...  68.7 us
    reduce_scatter x1, waiting for transfers between devices, shards(): lax.psum_scatter(lax.optimization_barrier(part_sum).astype(jnp.float32).a...  61.8 us
    all_gather x1, waiting for transfers between devices, shards(): part_rows = lax.all_gather(flat_rows, 'tp', axis=0, tiled=True)  52.6 us
    dot_general x32, matrix products, advance(): updated = values_in - jnp.dot(fix_rows, carried)  31.8 us
    dot_general x64, matrix products, advance(): output = jnp.dot(query_in, carried) + jnp.dot(score_in, updated)  31.7 us
    dot_general x32, matrix products, advance(): carried = carried * jnp.exp(total_in) + jnp.dot(key_in.T, updated)  24.8 us
  transfers between devices with their start and end apart: 4, of which 4 were waited for; matrix products, arithmetic and copies ran while one was open for 0% of the time, Pallas kernels for 0%

commit v1 on v0

--- a/solution.py
+++ b/solution.py
@@ -212,7 +212,13 @@
     source_count, slot_count, model_width = arrived.shape
     row_count = source_count * slot_count
     flat_rows = arrived.reshape(row_count, model_width)
-    part_rows = lax.all_gather(flat_rows, "tp", axis=0, tiled=True)
+    save_counts_by_axis = lambda u_in, array_axis: jnp.concatenate(
+        lax.all_to_all(
+            jnp.stack([u_in] * lax.axis_size("tp")), axis_name="tp", split_axis=0, concat_axis=0
+        ),
+        axis=array_axis,
+    )
+    part_rows = save_counts_by_axis(flat_rows, 0)
     gate_out = jnp.dot(part_rows, expert_gate[0], preferred_element_type=jnp.float32)
     up_out = jnp.dot(part_rows, expert_up[0], preferred_element_type=jnp.float32)
     hidden = (jax.nn.silu(gate_out) * up_out).astype(jnp.bfloat16)

time: 682 us -> 821 us (1.20)
  blocking collectives: 113 us -> 302 us
  waiting for transfers between devices: 192 us -> 136 us
    all_to_all x0 -> x1, blocking collectives: none -> 190 us  [shards(): lax.all_to_all(jnp.stack([u_in] * lax.axis_size('tp')), axis_name='tp', s...]
    all_gather x1 -> x0, waiting for transfers between devices: 52.6 us -> none  [shards(): part_rows = lax.all_gather(flat_rows, 'tp', axis=0, tiled=True)]
  transfers between devices with their start and end apart: 4 -> 3, of which waited for: 4 -> 3; matrix products, arithmetic and copies ran while one was open for 0% -> 0% of each run, Pallas kernels for 0% -> 0%
where the time goes in v1:
time: 821 us; the launch traced here: 814 us
  blocking collectives  302 us (37%)
  other arithmetic  171 us (21%)
  waiting for transfers between devices  136 us (17%)
  matrix products  130 us (16%)
  local copies, waits for them, and re-layouts  51.8 us (6%)
  between operations  14.4 us (2%)
    all_to_all x1, blocking collectives, shards(): lax.all_to_all(jnp.stack([u_in] * lax.axis_size('tp')), axis_name='tp', s...  190 us
    another operation x5, other arithmetic, block_sweep(): jax.scipy.linalg.solve_triangular(lower_matrix + identity, right_side, lo...  158 us
    all_gather x8, blocking collectives, prefix_by_axis(): lax.all_gather(part.astype(kind), axis)  96.7 us
    reduce_scatter x1, waiting for transfers between devices, shards(): lax.psum_scatter(lax.optimization_barrier(product).astype(jnp.float32).as...  65.8 us
    reduce_scatter x1, waiting for transfers between devices, shards(): lax.psum_scatter(lax.optimization_barrier(part_sum).astype(jnp.float32).a...  61.9 us
    dot_general x32, matrix products, advance(): updated = values_in - jnp.dot(fix_rows, carried)  31.8 us
    dot_general x64, matrix products, advance(): output = jnp.dot(query_in, carried) + jnp.dot(score_in, updated)  31.7 us
    dot_general x32, matrix products, advance(): carried = carried * jnp.exp(total_in) + jnp.dot(key_in.T, updated)  27 us
  transfers between devices with their start and end apart: 3, of which 3 were waited for; matrix products, arithmetic and copies ran while one was open for 0% of the time, Pallas kernels for 0%

profile of v1, /device:TPU:2, one launch (start us, length us, event | category | flops | bytes accessed | tf_op | source)
XLA Modules:
  0.0 814.4 jit_solution(12950232169389666617)
XLA Ops:
  12.5 78.6 %custom-call.6 = f32[1,16,1,64,64]{3,4,2,1,0:T(8,128)S(1)} custom-call(f32[1,16,1,64,64]{4,3,2,1,0:T(8,128)S(1)} %fusion.59), custom_call_target="InvertDiagBlocksLowerTriangular" | custom-call | tf_op jit(solution)/shard_map/vmap(jit(_solve_triangular))/vmap()/triangular_solve | solution.py:67
  101.5 3.4 rev.17
  107.4 79.4 %custom-call.7 = f32[1,16,1,64,64]{3,4,2,1,0:T(8,128)S(1)} custom-call(f32[1,16,1,64,64]{4,3,2,1,0:T(8,128)} %fusion.62), custom_call_target="InvertDiagBlocksLowerTriangular" | custom-call | tf_op jit(solution)/shard_map/vmap(jit(_solve_triangular))/vmap()/triangular_solve | solution.py:67
  192.9 54.0 %while.25 = (s32[]{:T(128)}, f32[1,128,256]{2,1,0:T(8,128)S(1)}, f32[16,1,64,256]{3,2,1,0:T(8,128)S(1)}, f32[16,1]{0,1:T(1,128)S(1)}, bf16[16,1,64,128]{3,2,1,0:...) while((s32[]{:T(128)}, f32[1,128,256]{2,1,0:T(8,128)S(1)}, ...), condition=%wide.region_7.9_spmd, body=%wide.region_6.8_spmd.sunk | while | flops 14794754 | bytes 952445 | solution.py:84
  250.0 57.1 %while.24 = (s32[]{:T(128)}, f32[1,128,256]{2,1,0:T(8,128)S(1)}, f32[16,1,64,256]{3,2,1,0:T(8,128)S(1)}, f32[16,1]{0,1:T(1,128)S(1)}, bf16[16,1,64,128]{3,2,1,0:...) while((s32[]{:T(128)}, f32[1,128,256]{2,1,0:T(8,128)S(1)}, ...), condition=%wide.region_4.6_spmd, body=%wide.region_3.5_spmd.sunk | while | flops 14794754 | bytes 952445 | solution.py:84
  307.1 12.1 %all-gather = bf16[4,128,128]{2,1,0:T(8,128)(2,1)S(1)} all-gather(bf16[1,128,128]{2,1,0:T(8,128)(2,1)S(1)} %get-tuple-element.234), channel_id=2, replica_groups=mesh['sp_0'=4,'sp_1'=4,'tp'=16] {'sp_1'}, dimensions={0}, use_global_device_ids=true | all-gather | bytes 163840 | tf_op jit(solution)/shard_map/all_gather | solution.py:26
  320.3 12.5 %all-gather.1 = bf16[512,128]{1,0:T(8,128)(2,1)S(1)} all-gather(bf16[128,128]{1,0:T(8,128)(2,1)S(1)} %fusion.226), channel_id=3, replica_groups=mesh['sp_0'=4,'sp_1'=4,'tp'=16] {'sp_0'}, dimensions={0}, use_global_device_ids=true | all-gather | bytes 163840 | tf_op jit(solution)/shard_map/all_gather | solution.py:26
  332.8 12.0 %all-gather.2 = bf16[4,128,128]{2,1,0:T(8,128)(2,1)S(1)} all-gather(bf16[1,128,128]{2,1,0:T(8,128)(2,1)S(1)} %get-tuple-element.235), channel_id=4, replica_groups=mesh['sp_0'=4,'sp_1'=4,'tp'=16] {'sp_1'}, dimensions={0}, use_global_device_ids=true | all-gather | bytes 163840 | tf_op jit(solution)/shard_map/all_gather | solution.py:26
  346.0 12.0 %all-gather.3 = bf16[512,128]{1,0:T(8,128)(2,1)S(1)} all-gather(bf16[128,128]{1,0:T(8,128)(2,1)S(1)} %convolution_add_fusion.15), channel_id=5, replica_groups=mesh['sp_0'=4,'sp_1'=4,'tp'=16] {'sp_0'}, dimensions={0}, use_global_device_ids=true | all-gather | bytes 163840 | tf_op jit(solution)/shard_map/all_gather | solution.py:26
  359.0 12.0 %all-gather.4 = bf16[4,128,128]{2,1,0:T(8,128)(2,1)S(1)} all-gather(bf16[1,128,128]{2,1,0:T(8,128)(2,1)S(1)} %get-tuple-element.236), channel_id=6, replica_groups=mesh['sp_0'=4,'sp_1'=4,'tp'=16] {'sp_1'}, dimensions={0}, use_global_device_ids=true | all-gather | bytes 163840 | tf_op jit(solution)/shard_map/all_gather | solution.py:26
  372.6 12.2 %all-gather.5 = bf16[512,128]{1,0:T(8,128)(2,1)S(1)} all-gather(bf16[128,128]{1,0:T(8,128)(2,1)S(1)} %fusion.229), channel_id=7, replica_groups=mesh['sp_0'=4,'sp_1'=4,'tp'=16] {'sp_0'}, dimensions={0}, use_global_device_ids=true | all-gather | bytes 163840 | tf_op jit(solution)/shard_map/all_gather | solution.py:26
  384.8 12.0 %all-gather.6 = bf16[4,128,128]{2,1,0:T(8,128)(2,1)S(1)} all-gather(bf16[1,128,128]{2,1,0:T(8,128)(2,1)S(1)} %get-tuple-element.237), channel_id=8, replica_groups=mesh['sp_0'=4,'sp_1'=4,'tp'=16] {'sp_1'}, dimensions={0}, use_global_device_ids=true | all-gather | bytes 163840 | tf_op jit(solution)/shard_map/all_gather | solution.py:26
  398.4 12.0 %all-gather.7 = bf16[512,128]{1,0:T(8,128)(2,1)S(1)} all-gather(bf16[128,128]{1,0:T(8,128)(2,1)S(1)} %convolution_add_fusion.6), channel_id=9, replica_groups=mesh['sp_0'=4,'sp_1'=4,'tp'=16] {'sp_0'}, dimensions={0}, use_global_device_ids=true | all-gather | bytes 163840 | tf_op jit(solution)/shard_map/all_gather | solution.py:26
  414.1 3.9 slice.185
  425.6 4.4 convolution_convert_fusion.1
  432.6 61.9 %reduce-scatter.3.cloned.1.call-done = bf16[64,2048]{1,0:T(8,128)(2,1)} async-done(((bf16[1024,2048]{1,0:T(8,128)(2,1)}), bf16[64,2048]{1,0:T(8,128)(2,1)}) %reduce-scatter.3.cloned.1.call-update) | async-done | bytes 262160 | tf_op jit(solution)/shard_map/reduce_scatter | solution.py:173
  497.0 15.8 %all_to_all.15 = bf16[16,8,2048]{2,1,0:T(8,128)(2,1)S(1)} all-to-all(bf16[16,8,2048]{2,1,0:T(8,128)(2,1)S(1)} %fusion.37), channel_id=1, replica_groups=mesh['sp_0'=4,'sp_1'=4,'tp'=16] {'sp_0','sp_1'}, dimensions={0} | all-to-all | bytes 1048576 | tf_op jit(solution)/shard_map/all_to_all | solution.py:211
  513.9 189.6 %all_to_all.16 = bf16[16,128,2048]{2,1,0:T(8,128)(2,1)S(1)} all-to-all(bf16[16,128,2048]{2,1,0:T(8,128)(2,1)S(1)} %stack.3), channel_id=1, replica_groups=mesh['sp_0'=4,'sp_1'=4,'tp'=16] {'tp'}, dimensions={0} | all-to-all | bytes 16777216 | tf_op jit(solution)/shard_map/all_to_all | solution.py:216
  703.5 3.2 copy-done.1
  706.7 2.4 fusion.86
  709.2 12.9 %convolution_convert_fusion = bf16[2048,2048]{1,0:T(8,128)(2,1)} fusion(bf16[2048,2048]{1,0:T(8,128)(2,1)} %bitcast.418, f32[2048,128]{1,0:T(8,128)S(1)} %fusion.86, bf16[1,2048,128]{2,1,0:T(8,128)(2,1)S(1)} %copy-done, bf16[1,2048,128]{2,1,0:T(8,128)(2,1)S(1)} %copy-done.7), kind=kOutput, calls=%fused_computation.46 | convolution fusion | flops 2153250816 | bytes 18874368 | tf_op jit(solution)/shard_map/dot_general | solution.py:225
  722.8 65.8 %reduce-scatter.5.cloned.1.call-done = bf16[128,2048]{1,0:T(8,128)(2,1)} async-done(((bf16[2048,2048]{1,0:T(8,128)(2,1)}), bf16[128,2048]{1,0:T(8,128)(2,1)}) %reduce-scatter.5.cloned.1.call-update) | async-done | bytes 524304 | tf_op jit(solution)/shard_map/reduce_scatter | solution.py:228
  788.5 7.3 all-to-all-start.2
  796.3 8.3 %all-to-all-done.2 = bf16[16,8,2048]{2,1,0:T(8,128)(2,1)S(1)} async-done(((bf16[16,8,2048]{2,1,0:T(8,128)(2,1)}), bf16[16,8,2048]{2,1,0:T(8,128)(2,1)S(1)}, u32[]{:S(2)}, u32[]{:S(2)}) %all-to-all-start.2) | async-done | bytes 524320 | tf_op jit(solution)/shard_map/all_to_all | solution.py:235
  (406 shorter events, 165.6 us)
Async XLA Ops:
  6.5 702.6 %copy-start = (bf16[1,2048,128]{2,1,0:T(8,128)(2,1)S(1)}, bf16[1,2048,128]{2,1,0:T(8,128)(2,1)}, u32[]{:S(2)}) copy-start(bf16[1,2048,128]{2,1,0:T(8,128)(2,1)} %param.41) | copy-start | bytes 1572868
  6.5 488.0 %reduce-scatter.3.cloned.1.call-start = ((), (), s32[]{:S(2)}) async-start(), calls=%async_computation.5 | async-start | bytes 4456448 | tf_op jit(solution)/shard_map/reduce_scatter | solution.py:173
  7.8 83.5 %copy-start.23 = (bf16[1024,1,128]{2,0,1:T(8,128)(2,1)S(1)}, bf16[1024,1,128]{2,0,1:T(8,128)(2,1)}, u32[]{:S(2)}) copy-start(bf16[1024,1,128]{2,0,1:T(8,128)(2,1)} %param.26) | copy-start | bytes 786436
  8.8 82.5 %copy-start.42 = (f32[64,64]{1,0:T(8,128)}, f32[64,64]{1,0:T(8,128)S(1)}, u32[]{:S(2)}) copy-start(f32[64,64]{1,0:T(8,128)S(1)} %get-tuple-element.256) | copy-start | bytes 49156
  8.8 82.5 %copy-start.48 = (pred[64,64]{1,0:T(8,128)(4,1)}, pred[64,64]{1,0:T(8,128)(4,1)S(1)}, u32[]{:S(2)}) copy-start(pred[64,64]{1,0:T(8,128)(4,1)S(1)} %get-tuple-element.255) | copy-start | bytes 12292
  8.9 82.5 %copy-start.43 = (f32[64,64]{1,0:T(8,128)}, f32[64,64]{1,0:T(8,128)S(1)}, u32[]{:S(2)}) copy-start(f32[64,64]{1,0:T(8,128)S(1)} %fusion.185) | copy-start | bytes 49156
  11.3 80.0 %copy-start.50 = (pred[64,64]{1,0:T(8,128)(4,1)}, pred[64,64]{1,0:T(8,128)(4,1)S(1)}, u32[]{:S(2)}) copy-start(pred[64,64]{1,0:T(8,128)(4,1)S(1)} %get-tuple-element.253) | copy-start | bytes 12292
  11.8 79.6 %copy-start.52 = (f32[16]{0:T(128)}, f32[16]{0:T(128)S(1)}, u32[]{:S(2)}) copy-start(f32[16]{0:T(128)S(1)} %slice_reduce_fusion.1) | copy-start | bytes 196
  105.3 81.7 %copy-start.54 = (f32[16]{0:T(128)}, f32[16]{0:T(128)S(1)}, u32[]{:S(2)}) copy-start(f32[16]{0:T(128)S(1)} %slice_reduce_fusion) | copy-start | bytes 196
  320.0 12.8 %copy-start.24 = (bf16[128,128]{1,0:T(8,128)(2,1)}, bf16[128,128]{1,0:T(8,128)(2,1)S(1)}, u32[]{:S(2)}) copy-start(bf16[128,128]{1,0:T(8,128)(2,1)S(1)} %fusion.228) | copy-start | bytes 98308
  320.1 12.7 %copy-start.26 = (bf16[128,128]{1,0:T(8,128)(2,1)}, bf16[128,128]{1,0:T(8,128)(2,1)S(1)}, u32[]{:S(2)}) copy-start(bf16[128,128]{1,0:T(8,128)(2,1)S(1)} %fusion.227) | copy-start | bytes 98308
  320.3 12.5 %copy-start.28 = (bf16[128,128]{1,0:T(8,128)(2,1)}, bf16[128,128]{1,0:T(8,128)(2,1)S(1)}, u32[]{:S(2)}) copy-start(bf16[128,128]{1,0:T(8,128)(2,1)S(1)} %fusion.226) | copy-start | bytes 98308
  344.9 27.1 %copy-start.11 = (bf16[128,128]{1,0:T(8,128)(2,1)}, bf16[128,128]{1,0:T(8,128)(2,1)S(1)}, u32[]{:S(2)}) copy-start(bf16[128,128]{1,0:T(8,128)(2,1)S(1)} %convolution_add_fusion.18) | copy-start | bytes 98308
  345.8 26.2 %copy-start.17 = (bf16[128,128]{1,0:T(8,128)(2,1)}, bf16[128,128]{1,0:T(8,128)(2,1)S(1)}, u32[]{:S(2)}) copy-start(bf16[128,128]{1,0:T(8,128)(2,1)S(1)} %convolution_add_fusion.16) | copy-start | bytes 98308
  346.0 26.1 %copy-start.13 = (bf16[128,128]{1,0:T(8,128)(2,1)}, bf16[128,128]{1,0:T(8,128)(2,1)S(1)}, u32[]{:S(2)}) copy-start(bf16[128,128]{1,0:T(8,128)(2,1)S(1)} %convolution_add_fusion.15) | copy-start | bytes 98308
  358.0 52.7 %copy-start.8 = (bf16[512,128]{1,0:T(8,128)(2,1)}, bf16[512,128]{1,0:T(8,128)(2,1)S(1)}, u32[]{:S(2)}) copy-start(bf16[512,128]{1,0:T(8,128)(2,1)S(1)} %all-gather.3) | copy-start | bytes 393220
  372.6 24.2 %copy-start.32 = (bf16[128,128]{1,0:T(8,128)(2,1)}, bf16[128,128]{1,0:T(8,128)(2,1)S(1)}, u32[]{:S(2)}) copy-start(bf16[128,128]{1,0:T(8,128)(2,1)S(1)} %fusion.229) | copy-start | bytes 98308
  384.8 27.9 %copy-start.9 = (bf16[512,128]{1,0:T(8,128)(2,1)}, bf16[512,128]{1,0:T(8,128)(2,1)S(1)}, u32[]{:S(2)}) copy-start(bf16[512,128]{1,0:T(8,128)(2,1)S(1)} %all-gather.5) | copy-start | bytes 393220
  430.0 358.6 %reduce-scatter.5.cloned.1.call-start = ((), (), s32[]{:S(2)}) async-start(), calls=%async_computation.6 | async-start | bytes 8912896 | tf_op jit(solution)/shard_map/reduce_scatter | solution.py:228
  431.1 63.4 %copy-start.2 = (bf16[64,2048]{1,0:T(8,128)(2,1)S(1)}, bf16[64,2048]{1,0:T(8,128)(2,1)}, u32[]{:S(2)}) copy-start(bf16[64,2048]{1,0:T(8,128)(2,1)} %param.34) | copy-start | bytes 786436
  431.1 64.6 %copy-start.47 = (f32[2048]{0:T(1024)S(1)}, f32[2048]{0:T(1024)}, u32[]{:S(2)}) copy-start(f32[2048]{0:T(1024)} %param.35) | copy-start | bytes 24580
  513.9 192.9 %copy-start.57 = (bf16[1,2048,128]{2,1,0:T(8,128)(2,1)S(1)}, bf16[1,2048,128]{2,1,0:T(8,128)(2,1)}, u32[]{:S(2)}) copy-start(bf16[1,2048,128]{2,1,0:T(8,128)(2,1)} %param.39) | copy-start | bytes 1572868
  722.1 73.8 %copy-start.56 = (f32[64,2]{0,1:T(2,128)S(1)}, f32[64,2]{0,1:T(2,128)}, u32[]{:S(2)}) copy-start(f32[64,2]{0,1:T(2,128)} %param.37) | copy-start | bytes 1540
  788.5 16.1 %all-to-all-start.2 = ((bf16[16,8,2048]{2,1,0:T(8,128)(2,1)}), bf16[16,8,2048]{2,1,0:T(8,128)(2,1)S(1)}, u32[]{:S(2)}, u32[]{:S(2)}) async-start(bf16[16,8,2048]{2,1,0:T(8,128)(2,1)} %bitcast.438), calls=%async_computation.4 | async-start | bytes 1048576 | tf_op jit(solution)/shard_map/all_to_all | solution.py:235
  (37 other events, 145.3 us)
Sparse Core Ops, SparseCore 0:
  430.1 64.3 reduce-scatter.2
  722.2 66.2 reduce-scatter.4
